TPU v7x, 256 devices: a whole 4x4x8 slice. The times are simulated.
256 devices in a mesh: sp: 64 (over z, y, core), tp: 4 (over x).
Axes of the slice: x: 4, y: 4, z: 8, core: 2. Of those that a mesh axis runs over, the one named last changes fastest.
Arguments:
- tokens: bfloat16 [49152, 2048], P('sp'), may hold values from -6 to 6
- input_gain: bfloat16 [2048], replicated, may hold values from 0.099609375 to 1.8984375
- gate_weight: bfloat16 [2048, 2048], P('sp', 'tp'), may hold values from -0.125 to 0.125
- value_weight: bfloat16 [2048, 2048], P('sp', 'tp'), may hold values from -0.125 to 0.125
- inflow_weight: bfloat16 [2048, 4, 128], P('sp', 'tp'), may hold values from -0.125 to 0.125
- readout_weight: bfloat16 [2048, 4, 128], P('sp', 'tp'), may hold values from -0.125 to 0.125
- step_weight: bfloat16 [2048, 2, 32], P('sp', None, 'tp'), may hold values from -0.125 to 0.125
- conv_values: bfloat16 [5, 2048], P(None, 'tp'), may hold values from -2.5 to 2.5
- conv_inflow: bfloat16 [5, 4, 128], P(None, 'tp'), may hold values from -2.5 to 2.5
- conv_readout: bfloat16 [5, 4, 128], P(None, 'tp'), may hold values from -2.5 to 2.5
- log_rate: float32 [2, 49152, 32], P(None, 'sp', 'tp'), may hold values from -20 to 0
- group_gain: bfloat16 [2048], P('tp'), may hold values from 0.099609375 to 1.8984375
- query_weight: bfloat16 [2048, 2048], P('sp', 'tp'), may hold values from -8 to 8
- key_weight: bfloat16 [2048, 512], P('sp', 'tp'), may hold values from -8 to 8
- vector_weight: bfloat16 [2048, 512], P('sp', 'tp'), may hold values from -0.125 to 0.125
- sink_logit: float32 [32], P('tp'), may hold values from 3 to 7
- state_out: bfloat16 [2048, 2048], P('tp', 'sp'), may hold values from -0.125 to 0.125
- window_out: bfloat16 [2048, 2048], P('tp', 'sp'), may hold values from -1 to 1
Outputs:
- mixed: bfloat16 [49152, 2048], P('sp', 'tp')
- log_total: float32 [49152, 32], P('sp', 'tp')
All inputs are finite; a program needn't handle non-finite values.
Results may differ from a plain program's by a relative error of at most 0.015.
The roundings to bfloat16 on the way count: a program that leaves them out, or rounds other values in their place, can miss the bound.
Values may be sent and summed in bfloat16 or wider, within the bound.
No kernel may reach another device: no remote copies, remote signals or barrier semaphores. Data moves between devices by JAX's collectives and lax.ppermute only.
A program may use at most 128 MiB of HBM per device.

v0:
```python
import jax
import jax.numpy as jnp
from jax import lax
from jax.sharding import Mesh
from jax.sharding import PartitionSpec as P

HEAD_DIM = 64
CONV = 5
SSD_BLOCK = 128
WINDOW = 128
QBLOCK = 256
GRID_W = 64
SP = ("sp_0", "sp_1", "sp_2")
EPS = 1e-06
ROPE_BASE = 10000.0
HIGH = lax.Precision.HIGH


def turned_gather(arrays, axis, dims):
    turned = [jnp.moveaxis(a, dim, 0) for a, dim in zip(arrays, dims)]
    widths = [t[0].size for t in turned]
    both = jnp.concatenate([t.reshape(-1, w) for t, w in zip(turned, widths)], axis=1)
    out = lax.all_gather(both, axis, axis=0, tiled=True)
    parts = jnp.split(out, [sum(widths[:k]) for k in range(1, len(widths))], axis=1)
    return tuple(
        (
            jnp.moveaxis(b.reshape(-1, *t.shape[1:]), 0, dim)
            for b, t, dim in zip(parts, turned, dims)
        )
    )


def nothing_yet(value, identity):
    return jax.tree.map(
        lambda part, zero: jnp.zeros_like(part) + jnp.asarray(zero, part.dtype), value, identity
    )


def carried_in(value, axes, combine, identity, reverse):
    before = start = nothing_yet(value, identity)
    running = value
    for axis in reversed(axes):
        length, position = (lax.axis_size(axis), lax.axis_index(axis))
        pieces = jax.tree.map(
            lambda part, kind: lax.all_gather(part.astype(kind), axis),
            running,
            jax.tree.map(lambda a: jnp.bfloat16 if a.dtype == jnp.float32 else a.dtype, value),
        )
        inside, running = (start, start)
        for k in reversed(range(length)) if reverse else range(length):
            passed = k > position if reverse else k < position
            running = combine(
                running, jax.tree.map(lambda part, own: part[k].astype(own.dtype), pieces, value)
            )
            inside = jax.tree.map(lambda new, old: jnp.where(passed, new, old), running, inside)
        before = combine(inside, before)
    return before


def with_halo(cells, sides, width):
    for axis, dim in sides:
        count = lax.axis_size(axis)
        ends = count - 1
        head = lax.slice_in_dim(cells, 0, width, axis=dim)
        tail = lax.slice_in_dim(cells, cells.shape[dim] - width, cells.shape[dim], axis=dim)
        cells = jnp.concatenate(
            [
                lax.ppermute(tail, axis, [(i, (i + 1) % count) for i in range(ends)]),
                cells,
                lax.ppermute(head, axis, [((i + 1) % count, i) for i in range(ends)]),
            ],
            axis=dim,
        )
    return cells


def cut_along(value, dim, length):
    shape = value.shape
    parts = value.reshape(*shape[:dim], length, shape[dim] // length, *shape[dim + 1 :])
    return jnp.moveaxis(parts, dim, 0)


def sent_and_summed(value, axis, dim):
    parts = cut_along(value, dim, lax.axis_size(axis))
    arrived = lax.all_to_all(parts, axis, split_axis=0, concat_axis=0, tiled=True)
    return arrived.astype(jnp.float32).sum(axis=0)


def rope_pairs(part, angle):
    half = part.shape[-1] // 2
    cosine = jnp.cos(angle)[:, None, :]
    sine = jnp.sin(angle)[:, None, :]
    first = part[..., :half]
    second = part[..., half:]
    return jnp.concatenate(
        [first * cosine - second * sine, second * cosine + first * sine], axis=-1
    )


def axial_rope(heads, positions):
    width = heads.shape[-1]
    quarter = width // 4
    freqs = ROPE_BASE ** (-jnp.arange(quarter).astype(jnp.float32) / quarter)
    row_angle = (positions // GRID_W).astype(jnp.float32)[:, None] * freqs
    col_angle = (positions % GRID_W).astype(jnp.float32)[:, None] * freqs
    half = width // 2
    wide = heads.astype(jnp.float32)
    turned = jnp.concatenate(
        [rope_pairs(wide[..., :half], row_angle), rope_pairs(wide[..., half:], col_angle)], axis=-1
    )
    return turned.astype(jnp.bfloat16)


def block_ssd(state, inputs):
    xdt, decay, inflow, readout = inputs
    length = decay.shape[0]
    heads = xdt.shape[1]
    groups = inflow.shape[1]
    repeat = heads // groups
    cum = jnp.cumsum(decay, axis=0)
    seg = cum[:, None, :] - cum[None, :, :]
    lower = jnp.arange(length)[:, None] >= jnp.arange(length)[None, :]
    weight = jnp.exp(jnp.where(lower[:, :, None], seg, -jnp.inf))
    intersection = jnp.einsum("lgn,sgn->lsg", readout, inflow, preferred_element_type=jnp.float32)
    intersection = jnp.repeat(intersection, repeat, axis=2)
    final_result = jnp.einsum("lsh,shp->lhp", intersection * weight, xdt, precision=HIGH)
    read_heads = jnp.repeat(readout, repeat, axis=1).astype(jnp.float32)
    final_result = final_result + jnp.exp(cum)[:, :, None] * jnp.einsum(
        "lhn,hpn->lhp", read_heads, state, precision=HIGH
    )
    write_heads = jnp.repeat(inflow, repeat, axis=1).astype(jnp.float32)
    to_end = jnp.exp(cum[-1][None, :] - cum)
    fresh = jnp.einsum("shp,shn->hpn", xdt * to_end[:, :, None], write_heads, precision=HIGH)
    return (jnp.exp(cum[-1])[:, None, None] * state + fresh, final_result)


def chain(earlier, later):
    return (earlier[0] + later[0], jnp.exp(later[0])[:, None, None] * earlier[1] + later[1])


def flatten_rows(weight):
    return weight.reshape(weight.shape[0], -1)


def shards(
    tokens,
    input_gain,
    gate_weight,
    value_weight,
    inflow_weight,
    readout_weight,
    step_weight,
    conv_values,
    conv_inflow,
    conv_readout,
    log_rate,
    group_gain,
    query_weight,
    key_weight,
    vector_weight,
    sink_logit,
    state_out,
    window_out,
):
    count = tokens.shape[0]
    offset = lax.axis_index(SP) * count
    seq_total = count * lax.axis_size(SP)
    positions = offset + jnp.arange(count, dtype=jnp.int32)
    heads = step_weight.shape[2]
    groups = inflow_weight.shape[1]
    state_len = inflow_weight.shape[2]
    inner_local = value_weight.shape[1]
    q_count = query_weight.shape[1] // HEAD_DIM
    kv_count = key_weight.shape[1] // HEAD_DIM
    kv_width = key_weight.shape[1]
    wide = tokens.astype(jnp.float32)
    normed = (
        wide
        * lax.rsqrt(jnp.mean(wide * wide, axis=1, keepdims=True) + EPS)
        * input_gain.astype(jnp.float32)
    ).astype(jnp.bfloat16)
    out_stack = jnp.concatenate([state_out, window_out], axis=0)
    gathered = turned_gather(
        (
            gate_weight,
            value_weight,
            inflow_weight,
            readout_weight,
            step_weight,
            query_weight,
            key_weight,
            vector_weight,
            out_stack,
        ),
        SP,
        (0, 0, 0, 0, 0, 0, 0, 0, 1),
    )
    pieces = gathered[:8]
    matrices = (
        pieces[0],
        jnp.concatenate([pieces[1], flatten_rows(pieces[2]), flatten_rows(pieces[3])], axis=1),
        flatten_rows(pieces[4]),
        pieces[5],
        jnp.concatenate([pieces[6], pieces[7]], axis=1),
    )
    sums = tuple(
        (jnp.dot(normed, matrix, preferred_element_type=jnp.float32) for matrix in matrices)
    )
    out_whole = gathered[8]
    gate = sums[0].astype(jnp.bfloat16)
    conv_input = sums[1].astype(jnp.bfloat16)
    step = jax.nn.softplus(sums[2]).reshape(count, 2, heads)
    queries = sums[3].astype(jnp.bfloat16)
    keyvals = sums[4].astype(jnp.bfloat16)

    def direction(xdt, decay, inflow, readout, backward):
        if backward:
            xdt = jnp.flip(xdt, 0)
            decay = jnp.flip(decay, 0)
            inflow = jnp.flip(inflow, 0)
            readout = jnp.flip(readout, 0)
        blocks = count // SSD_BLOCK
        start_state = jnp.zeros((heads, HEAD_DIM, state_len), jnp.float32)
        shaped = (
            xdt.reshape(blocks, SSD_BLOCK, heads, HEAD_DIM),
            decay.reshape(blocks, SSD_BLOCK, heads),
            inflow.reshape(blocks, SSD_BLOCK, groups, state_len),
            readout.reshape(blocks, SSD_BLOCK, groups, state_len),
        )
        end_state, local = lax.scan(block_ssd, start_state, shaped)
        local = local.reshape(count, heads, HEAD_DIM)
        summary = (jnp.sum(decay, axis=0), end_state)
        identity = (jnp.zeros((heads,), jnp.float32), jnp.zeros_like(end_state))
        if backward:
            incoming = carried_in(summary, SP, chain, identity, True)
        else:
            incoming = carried_in(summary, SP, chain, identity, False)
        reach = jnp.exp(jnp.cumsum(decay, axis=0))
        per_head = jnp.repeat(readout, heads // groups, axis=1).astype(jnp.float32)
        local = local + reach[:, :, None] * jnp.einsum(
            "lhn,hpn->lhp", per_head, incoming[1], precision=HIGH
        )
        if backward:
            local = jnp.flip(local, 0)
        return local

    reach_rows = CONV // 2
    padded = with_halo(conv_input, ((SP, 0),), CONV // 2).astype(jnp.float32)
    taps = jnp.concatenate(
        [conv_values, flatten_rows(conv_inflow), flatten_rows(conv_readout)], axis=1
    ).astype(jnp.float32)
    conv_sum = padded[0:count] * taps[0]
    for tap in range(1, 2 * reach_rows + 1):
        conv_sum = conv_sum + padded[tap : tap + count] * taps[tap]
    conv_short = jax.nn.silu(conv_sum).astype(jnp.bfloat16)
    conv_out = conv_short.astype(jnp.float32)
    split_mid = inner_local + groups * state_len
    xs = conv_out[:, :inner_local].reshape(count, heads, HEAD_DIM)
    inflow = conv_short[:, inner_local:split_mid].reshape(count, groups, state_len)
    readout = conv_short[:, split_mid:].reshape(count, groups, state_len)
    decay = -jnp.exp(log_rate) * jnp.transpose(step, (1, 0, 2))
    forward = direction(xs * step[:, 0, :, None], decay[0], inflow, readout, False)
    backward = direction(xs * step[:, 1, :, None], decay[1], inflow, readout, True)
    combined = (forward + backward).reshape(count, -1) * jax.nn.silu(gate.astype(jnp.float32))
    grouped = combined.reshape(count, groups, -1)
    grouped = grouped * lax.rsqrt(jnp.mean(grouped * grouped, axis=2, keepdims=True) + EPS)
    state_features = (grouped.reshape(count, -1) * group_gain.astype(jnp.float32)).astype(
        jnp.bfloat16
    )
    q_heads = axial_rope(queries.reshape(count, q_count, HEAD_DIM), positions)
    k_heads = axial_rope(keyvals[:, :kv_width].reshape(count, kv_count, HEAD_DIM), positions)
    both = jnp.concatenate([k_heads.reshape(count, -1), keyvals[:, kv_width:]], axis=1)
    beside_all = with_halo(both, ((SP, 0),), WINDOW)
    repeat = q_count // kv_count
    band = QBLOCK + 2 * WINDOW
    sinks = sink_logit.reshape(kv_count, repeat, 1, 1)
    grouped_q = q_heads.reshape(count, kv_count, repeat, HEAD_DIM)

    def attend(index):
        start = index * QBLOCK
        block_q = lax.dynamic_slice_in_dim(grouped_q, start, QBLOCK, 0)
        block_kv = lax.dynamic_slice_in_dim(beside_all, start, band, 0)
        block_k = block_kv[:, :kv_width].reshape(band, kv_count, HEAD_DIM)
        block_v = block_kv[:, kv_width:].reshape(band, kv_count, HEAD_DIM)
        scores = jnp.einsum(
            "qkrd,skd->krqs", block_q, block_k, preferred_element_type=jnp.float32
        ) * HEAD_DIM ** (-0.5)
        query_pos = offset + start + jnp.arange(QBLOCK, dtype=jnp.int32)
        key_pos = offset + start - WINDOW + jnp.arange(band, dtype=jnp.int32)
        valid = (
            (jnp.abs(query_pos[:, None] - key_pos[None, :]) <= WINDOW)
            & (key_pos >= 0)[None, :]
            & (key_pos < seq_total)[None, :]
        )
        scores = jnp.where(valid, scores, -jnp.inf)
        top = jnp.maximum(jnp.max(scores, axis=-1, keepdims=True), sinks)
        expo = jnp.exp(scores - top)
        total = jnp.sum(expo, axis=-1, keepdims=True) + jnp.exp(sinks - top)
        probs = expo.astype(jnp.bfloat16)
        values = jnp.einsum("krqs,skd->qkrd", probs, block_v, preferred_element_type=jnp.float32)
        values = values / jnp.transpose(total, (2, 0, 1, 3))
        logs = jnp.transpose((top + jnp.log(total))[..., 0], (2, 0, 1)).reshape(QBLOCK, -1)
        return (values.astype(jnp.bfloat16).reshape(QBLOCK, -1), logs)

    feats, logs = lax.map(attend, jnp.arange(count // QBLOCK, dtype=jnp.int32))
    window_features = feats.reshape(count, -1)
    log_total = logs.reshape(count, -1)
    features = jnp.concatenate([state_features, window_features], axis=1)
    terms = jnp.dot(features, out_whole, preferred_element_type=jnp.float32)
    mixed = sent_and_summed(terms.astype(jnp.bfloat16), "tp", 1).astype(jnp.bfloat16)
    return (mixed, log_total)


def solution(mesh):
    torus = Mesh(mesh.devices.reshape(8, 4, 2, mesh.shape["tp"]), ("sp_0", "sp_1", "sp_2", "tp"))
    return jax.shard_map(
        shards,
        mesh=torus,
        in_specs=(
            P(SP, None),
            P(),
            P(SP, "tp"),
            P(SP, "tp"),
            P(SP, "tp", None),
            P(SP, "tp", None),
            P(SP, None, "tp"),
            P(None, "tp"),
            P(None, "tp", None),
            P(None, "tp", None),
            P(None, SP, "tp"),
            P("tp"),
            P(SP, "tp"),
            P(SP, "tp"),
            P(SP, "tp"),
            P("tp"),
            P("tp", SP),
            P("tp", SP),
        ),
        out_specs=(P(SP, "tp"), P(SP, "tp")),
        check_vma=False,
    )
```

profile of v0, /device:TPU:8, one launch (start us, length us, event | category | flops | bytes accessed | tf_op | source)
XLA Modules:
  0.0 523.0 jit_solution(13843516485455394829)
XLA Ops:
  19.3 83.6 %all-gather.12.cloned.1.call-done = bf16[2048,3088]{1,0:T(8,128)(2,1)} async-done(((bf16[32,3088]{1,0:T(8,128)(2,1)}), bf16[2048,3088]{1,0:T(8,128)(2,1)}) %all-gather.12.cloned.1.call-update) | async-done | bytes 12648464 | tf_op jit(solution)/shard_map/all_gather | solution.py:23
  102.9 4.1 convolution_convert_fusion
  113.4 4.6 fusion.107
  121.5 5.5 %fusion.101 = bf16[768,768]{1,0:T(8,128)(2,1)S(1)} fusion(bf16[2048,3088]{1,0:T(8,128)(2,1)} %all-gather.12.cloned.1.call-done, bf16[768,2048]{1,0:T(8,128)(2,1)} %param.24, f32[2048]{0:T(1024)S(1)} %convert_element_type.661, f32[768]{0:T(1024)S(1)} %add_rsqrt_fusion.1), kind=kOutput, calls=%fused_computation.141 | convolution fusion | flops 2422800384 | bytes 7482368 | tf_op jit(solution)/shard_map/dot_general | solution.py:207
  127.0 3.6 collective-permute-start.1
  139.2 10.6 %all-gather.6 = bf16[4,1,8]{2,1,0:T(2,128)(2,1)S(1)} all-gather(bf16[1,1,8]{2,1,0:T(2,128)(2,1)S(1)} %get-tuple-element.405), channel_id=1, replica_groups=mesh['sp_0'=8,'sp_1'=4,'sp_2'=2,'tp'=4] {'sp_1'}, dimensions={0}, use_global_device_ids=true | all-gather | bytes 80 | tf_op jit(solution)/shard_map/all_gather | solution.py:45
  151.5 16.1 %all-gather.7 = bf16[8,1,8]{2,1,0:T(2,128)(2,1)S(1)} all-gather(bf16[1,1,8]{2,1,0:T(2,128)(2,1)S(1)} %get-tuple-element.396), channel_id=1, replica_groups=mesh['sp_0'=8,'sp_1'=4,'sp_2'=2,'tp'=4] {'sp_0'}, dimensions={0}, use_global_device_ids=true | all-gather | bytes 144 | tf_op jit(solution)/shard_map/all_gather | solution.py:45
  171.6 10.2 %all-gather.4 = bf16[4,1,8]{2,1,0:T(2,128)(2,1)S(1)} all-gather(bf16[1,1,8]{2,1,0:T(2,128)(2,1)S(1)} %get-tuple-element.402), channel_id=1, replica_groups=mesh['sp_0'=8,'sp_1'=4,'sp_2'=2,'tp'=4] {'sp_1'}, dimensions={0}, use_global_device_ids=true | all-gather | bytes 80 | tf_op jit(solution)/shard_map/all_gather | solution.py:45
  183.6 13.5 %all-gather.5 = bf16[8,1,8]{2,1,0:T(2,128)(2,1)S(1)} all-gather(bf16[1,1,8]{2,1,0:T(2,128)(2,1)S(1)} %get-tuple-element.391), channel_id=1, replica_groups=mesh['sp_0'=8,'sp_1'=4,'sp_2'=2,'tp'=4] {'sp_0'}, dimensions={0}, use_global_device_ids=true | all-gather | bytes 144 | tf_op jit(solution)/shard_map/all_gather | solution.py:45
  222.3 74.4 %while.42 = (s32[]{:T(128)}, f32[8,64,128]{2,1,0:T(8,128)S(1)}, f32[6,128,8,64]{1,0,3,2:T(8,128)S(1)}, f32[6,128,8]{2,1,0:T(8,128)}, f32[6,128,8,64]{1,0,3,2:T(8...) while((s32[]{:T(128)}, f32[8,64,128]{2,1,0:T(8,128)S(1)}, ...), condition=%wide.region_9.10_spmd.clone, body=%wide.region_7.9_spmd.clone.sunk | while | flops 156188672 | bytes 3768652 | solution.py:230
  229.6 5.1 dynamic_update_slice.32
  242.0 5.1 dynamic_update_slice.32
  254.4 5.1 dynamic_update_slice.32
  266.8 5.1 dynamic_update_slice.32
  279.2 5.1 dynamic_update_slice.32
  291.6 5.1 dynamic_update_slice.32
  299.6 11.9 %all_gather.68 = bf16[4,8,64,128]{3,2,1,0:T(8,128)(2,1)S(1)} all-gather(bf16[1,8,64,128]{3,2,1,0:T(8,128)(2,1)S(1)} %fusion.172), channel_id=1, replica_groups=mesh['sp_0'=8,'sp_1'=4,'sp_2'=2,'tp'=4] {'sp_1'}, dimensions={0}, use_global_device_ids=true | all-gather | bytes 655360 | tf_op jit(solution)/shard_map/all_gather | solution.py:45
  318.4 80.1 %while.41 = (s32[]{:T(128)}, f32[8,64,128]{2,1,0:T(8,128)S(1)}, f32[6,128,8,64]{1,0,3,2:T(8,128)}, f32[6,128,8]{2,1,0:T(8,128)}, f32[6,128,8,64]{1,0,3,2:T(8,128...) while((s32[]{:T(128)}, f32[8,64,128]{2,1,0:T(8,128)S(1)}, ...), condition=%wide.region_3.4_spmd.clone, body=%wide.region_1.3_spmd.clone.sunk | while | flops 156188672 | bytes 3768652 | solution.py:230
  324.1 7.7 %dynamic_update_slice.31 = f32[6,128,8,64]{1,0,3,2:T(8,128)} dynamic-update-slice(f32[6,128,8,64]{1,0,3,2:T(8,128)} %get-tuple-element.665, f32[1,128,8,64]{1,0,3,2:T(1,128)S(1)} %bitcast.674, s32[]{:T(128)S(6)} %copy.178, s32[]{:T(128)} %constant.172.clone.1..sunk.1, s32[]{:T(128)} %constant.172.clone.1..sunk.1, s32[]{:T(128)} %constant.172.clone.1..sunk.1) | dynamic-update-slice | bytes 524292 | tf_op jit(solution)/shard_map/while/body/jit(dynamic_update_index_in_dim)/dynamic_update_slice | solution.py:230
  337.4 7.7 %dynamic_update_slice.31 = f32[6,128,8,64]{1,0,3,2:T(8,128)} dynamic-update-slice(f32[6,128,8,64]{1,0,3,2:T(8,128)} %get-tuple-element.665, f32[1,128,8,64]{1,0,3,2:T(1,128)S(1)} %bitcast.674, s32[]{:T(128)S(6)} %copy.178, s32[]{:T(128)} %constant.172.clone.1..sunk.1, s32[]{:T(128)} %constant.172.clone.1..sunk.1, s32[]{:T(128)} %constant.172.clone.1..sunk.1) | dynamic-update-slice | bytes 524292 | tf_op jit(solution)/shard_map/while/body/jit(dynamic_update_index_in_dim)/dynamic_update_slice | solution.py:230
  350.8 7.7 %dynamic_update_slice.31 = f32[6,128,8,64]{1,0,3,2:T(8,128)} dynamic-update-slice(f32[6,128,8,64]{1,0,3,2:T(8,128)} %get-tuple-element.665, f32[1,128,8,64]{1,0,3,2:T(1,128)S(1)} %bitcast.674, s32[]{:T(128)S(6)} %copy.178, s32[]{:T(128)} %constant.172.clone.1..sunk.1, s32[]{:T(128)} %constant.172.clone.1..sunk.1, s32[]{:T(128)} %constant.172.clone.1..sunk.1) | dynamic-update-slice | bytes 524292 | tf_op jit(solution)/shard_map/while/body/jit(dynamic_update_index_in_dim)/dynamic_update_slice | solution.py:230
  364.1 7.7 %dynamic_update_slice.31 = f32[6,128,8,64]{1,0,3,2:T(8,128)} dynamic-update-slice(f32[6,128,8,64]{1,0,3,2:T(8,128)} %get-tuple-element.665, f32[1,128,8,64]{1,0,3,2:T(1,128)S(1)} %bitcast.674, s32[]{:T(128)S(6)} %copy.178, s32[]{:T(128)} %constant.172.clone.1..sunk.1, s32[]{:T(128)} %constant.172.clone.1..sunk.1, s32[]{:T(128)} %constant.172.clone.1..sunk.1) | dynamic-update-slice | bytes 524292 | tf_op jit(solution)/shard_map/while/body/jit(dynamic_update_index_in_dim)/dynamic_update_slice | solution.py:230
  377.5 7.7 %dynamic_update_slice.31 = f32[6,128,8,64]{1,0,3,2:T(8,128)} dynamic-update-slice(f32[6,128,8,64]{1,0,3,2:T(8,128)} %get-tuple-element.665, f32[1,128,8,64]{1,0,3,2:T(1,128)S(1)} %bitcast.674, s32[]{:T(128)S(6)} %copy.178, s32[]{:T(128)} %constant.172.clone.1..sunk.1, s32[]{:T(128)} %constant.172.clone.1..sunk.1, s32[]{:T(128)} %constant.172.clone.1..sunk.1) | dynamic-update-slice | bytes 524292 | tf_op jit(solution)/shard_map/while/body/jit(dynamic_update_index_in_dim)/dynamic_update_slice | solution.py:230
  390.8 7.7 %dynamic_update_slice.31 = f32[6,128,8,64]{1,0,3,2:T(8,128)} dynamic-update-slice(f32[6,128,8,64]{1,0,3,2:T(8,128)} %get-tuple-element.665, f32[1,128,8,64]{1,0,3,2:T(1,128)S(1)} %bitcast.674, s32[]{:T(128)S(6)} %copy.178, s32[]{:T(128)} %constant.172.clone.1..sunk.1, s32[]{:T(128)} %constant.172.clone.1..sunk.1, s32[]{:T(128)} %constant.172.clone.1..sunk.1) | dynamic-update-slice | bytes 524292 | tf_op jit(solution)/shard_map/while/body/jit(dynamic_update_index_in_dim)/dynamic_update_slice | solution.py:230
  402.0 13.7 %all_gather.61 = bf16[4,8,64,128]{3,2,1,0:T(8,128)(2,1)S(1)} all-gather(bf16[1,8,64,128]{3,2,1,0:T(8,128)(2,1)S(1)} %fusion.168), channel_id=1, replica_groups=mesh['sp_0'=8,'sp_1'=4,'sp_2'=2,'tp'=4] {'sp_1'}, dimensions={0}, use_global_device_ids=true | all-gather | bytes 655360 | tf_op jit(solution)/shard_map/all_gather | solution.py:45
  422.7 19.3 %while.40 = (s32[]{:T(128)}, bf16[3,256,512]{2,1,0:T(8,128)(2,1)S(1)}, f32[3,256,8]{1,2,0:T(8,128)}, s32[3]{0:T(128)S(1)}, bf16[1024,256]{0,1:T(8,128)(2,1)S(1)}...) while((s32[]{:T(128)}, ...), condition=%wide.region_17.18_spmd, body=%wide.region_14.17_spmd.sunk | while | flops 280901888 | bytes 15614348 | solution.py:305
  443.3 4.5 fusion.98
  448.0 5.0 rev.16
  453.0 7.5 %all-gather.14.cloned.1.call-done = bf16[8,8,64,128]{3,2,1,0:T(8,128)(2,1)} async-done(((bf16[1,8,64,128]{3,2,1,0:T(8,128)(2,1)}), bf16[8,8,64,128]{3,2,1,0:T(8,128)(2,1)}) %all-gather.14.cloned.1.call-update) | async-done | bytes 1048592 | tf_op jit(solution)/shard_map/all_gather | solution.py:45
  464.0 4.0 multiply_reduce_fusion
  469.1 8.7 %fusion.78 = bf16[768,2048]{1,0:T(8,128)(2,1)S(1)} fusion(bf16[2048,3088]{1,0:T(8,128)(2,1)} %all-gather.12.cloned.1.call-done, bf16[768,512]{0,1:T(8,128)(2,1)S(1)} %copy-done.11, bf16[768,512]{0,1:T(8,128)(2,1)S(1)} %multiply_convert_fusion.1), kind=kOutput, calls=%fused_computation.107 | convolution fusion | flops 3225944064 | bytes 8912896 | tf_op jit(solution)/shard_map/dot_general | solution.py:309
  478.1 36.8 %all_to_all.5 = bf16[4,768,512]{2,1,0:T(8,128)(2,1)S(1)} all-to-all(bf16[4,768,512]{2,1,0:T(8,128)(2,1)S(1)} %bitcast.677), channel_id=1, replica_groups=mesh['sp_0'=8,'sp_1'=4,'sp_2'=2,'tp'=4] {'tp'}, dimensions={0} | all-to-all | bytes 6291456 | tf_op jit(solution)/shard_map/all_to_all | solution.py:85
  (447 shorter events, 184.1 us)
Async XLA Ops:
  7.2 95.8 %all-gather.12.cloned.1.call-start = ((), (), s32[]{:S(2)}) async-start(), calls=%async_computation.1 | async-start | bytes 13312000 | tf_op jit(solution)/shard_map/all_gather | solution.py:23
  10.4 432.7 %all-gather.16.cloned.1.call-start = ((), (), s32[]{:S(2)}) async-start(), calls=%async_computation.3 | async-start | bytes 1179648 | tf_op jit(solution)/shard_map/all_gather | solution.py:45
  18.9 102.6 %copy-start.16 = (f32[768]{0:T(1024)}, f32[768]{0:T(1024)S(1)}, u32[]{:S(2)}) copy-start(f32[768]{0:T(1024)S(1)} %add_rsqrt_fusion.1) | copy-start | bytes 9220
  107.9 313.6 %collective-permute-start.3 = (bf16[128,256]{0,1:T(8,128)(2,1)}, bf16[128,256]{0,1:T(8,128)(2,1)}, u32[]{:S(2)}, u32[]{:S(2)}) collective-permute-start(bf16[128,256]{0,1:T(8,128)(2,1)} %get-tuple-element.360), channel_id=1, source_target_pairs={{4,0},{8,4},{12,8},{16,12},{20,16},{24,20},{28,24},{32,28},{36,32}... | collective-permute-start | bytes 196616 | tf_op jit(solution)/shard_map/ppermute | solution.py:70
  111.4 310.1 %collective-permute-start.2 = (bf16[128,256]{0,1:T(8,128)(2,1)}, bf16[128,256]{0,1:T(8,128)(2,1)}, u32[]{:S(2)}, u32[]{:S(2)}) collective-permute-start(bf16[128,256]{0,1:T(8,128)(2,1)} %get-tuple-element.359), channel_id=1, source_target_pairs={{0,4},{4,8},{8,12},{12,16},{16,20},{20,24},{24,28},{28,32},{32,36}... | collective-permute-start | bytes 196616 | tf_op jit(solution)/shard_map/ppermute | solution.py:68
  127.0 74.1 %collective-permute-start.1 = (bf16[2,768]{1,0:T(2,128)(2,1)S(1)}, bf16[2,768]{1,0:T(2,128)(2,1)S(1)}, u32[]{:S(2)}, u32[]{:S(2)}) collective-permute-start(bf16[2,768]{1,0:T(2,128)(2,1)S(1)} %get-tuple-element.354), channel_id=1, source_target_pairs={{4,0},{8,4},{12,8},{16,12},{20,16},{24,20},{28,24},{32,28},{36,32}... | collective-permute-start | bytes 9224 | tf_op jit(solution)/shard_map/ppermute | solution.py:70
  130.6 70.5 %collective-permute-start = (bf16[2,768]{1,0:T(2,128)(2,1)S(1)}, bf16[2,768]{1,0:T(2,128)(2,1)S(1)}, u32[]{:S(2)}, u32[]{:S(2)}) collective-permute-start(bf16[2,768]{1,0:T(2,128)(2,1)S(1)} %get-tuple-element.353), channel_id=1, source_target_pairs={{0,4},{4,8},{8,12},{12,16},{16,20},{20,24},{24,28},{28,32},{32,36}... | collective-permute-start | bytes 9224 | tf_op jit(solution)/shard_map/ppermute | solution.py:68
  296.7 17.2 %copy-start.12 = (f32[6,128,8]{1,0,2:T(8,128)S(1)}, f32[6,128,8]{1,0,2:T(8,128)}, u32[]{:S(2)}) copy-start(f32[6,128,8]{1,0,2:T(8,128)} %copy.92) | copy-start | bytes 73732
  298.7 18.2 %copy-start.6 = (bf16[16,64,128]{2,1,0:T(8,128)(2,1)}, bf16[16,64,128]{2,1,0:T(8,128)(2,1)S(1)}, u32[]{:S(2)}) copy-start(bf16[16,64,128]{2,1,0:T(8,128)(2,1)S(1)} %all-gather.3) | copy-start | bytes 786436
  313.8 146.7 %all-gather.14.cloned.1.call-start = ((), (), s32[]{:S(2)}) async-start(), calls=%async_computation.2 | async-start | bytes 1179648 | tf_op jit(solution)/shard_map/all_gather | solution.py:45
  422.5 20.7 %copy-start.7 = (bf16[16,64,128]{2,1,0:T(8,128)(2,1)S(1)}, bf16[16,64,128]{2,1,0:T(8,128)(2,1)}, u32[]{:S(2)}) copy-start(bf16[16,64,128]{2,1,0:T(8,128)(2,1)} %copy-done.6) | copy-start | bytes 786436
  422.5 20.7 %copy-start.13 = (f32[768,8]{0,1:T(8,128)S(1)}, f32[768,8]{0,1:T(8,128)}, u32[]{:S(2)}) copy-start(f32[768,8]{0,1:T(8,128)} %exponential_bitcast_fusion) | copy-start | bytes 73732
  422.5 20.7 %copy-start.20 = (f32[8]{0:T(128)S(1)}, f32[8]{0:T(128)}, u32[]{:S(2)}) copy-start(f32[8]{0:T(128)} %get-tuple-element.404) | copy-start | bytes 100
  422.5 20.6 %copy-start.21 = (f32[8]{0:T(128)S(1)}, f32[8]{0:T(128)}, u32[]{:S(2)}) copy-start(f32[8]{0:T(128)} %get-tuple-element.406) | copy-start | bytes 100
  422.5 20.6 %copy-start.23 = (f32[8]{0:T(128)S(1)}, f32[8]{0:T(128)}, u32[]{:S(2)}) copy-start(f32[8]{0:T(128)} %get-tuple-element.397) | copy-start | bytes 100
  422.5 20.6 %copy-start.27 = (f32[8]{0:T(128)S(1)}, f32[8]{0:T(128)}, u32[]{:S(2)}) copy-start(f32[8]{0:T(128)} %get-tuple-element.398) | copy-start | bytes 100
  422.6 20.6 %copy-start.28 = (f32[8]{0:T(128)S(1)}, f32[8]{0:T(128)}, u32[]{:S(2)}) copy-start(f32[8]{0:T(128)} %get-tuple-element.399) | copy-start | bytes 100
  422.6 20.6 %copy-start.29 = (f32[8]{0:T(128)S(1)}, f32[8]{0:T(128)}, u32[]{:S(2)}) copy-start(f32[8]{0:T(128)} %get-tuple-element.400) | copy-start | bytes 100
  422.6 20.6 %copy-start.31 = (f32[8]{0:T(128)S(1)}, f32[8]{0:T(128)}, u32[]{:S(2)}) copy-start(f32[8]{0:T(128)} %get-tuple-element.329) | copy-start | bytes 100
  422.6 20.6 %copy-start.40 = (f32[8]{0:T(128)S(1)}, f32[8]{0:T(128)}, u32[]{:S(2)}) copy-start(f32[8]{0:T(128)} %get-tuple-element.383) | copy-start | bytes 100
  422.6 20.6 %copy-start.41 = (f32[8]{0:T(128)S(1)}, f32[8]{0:T(128)}, u32[]{:S(2)}) copy-start(f32[8]{0:T(128)} %get-tuple-element.384) | copy-start | bytes 100
  422.6 20.6 %copy-start.42 = (f32[8]{0:T(128)S(1)}, f32[8]{0:T(128)}, u32[]{:S(2)}) copy-start(f32[8]{0:T(128)} %get-tuple-element.385) | copy-start | bytes 100
  422.6 20.6 %copy-start.43 = (f32[8]{0:T(128)S(1)}, f32[8]{0:T(128)}, u32[]{:S(2)}) copy-start(f32[8]{0:T(128)} %get-tuple-element.386) | copy-start | bytes 100
  422.6 20.6 %copy-start.44 = (f32[8]{0:T(128)S(1)}, f32[8]{0:T(128)}, u32[]{:S(2)}) copy-start(f32[8]{0:T(128)} %get-tuple-element.387) | copy-start | bytes 100
  422.6 20.6 %copy-start.45 = (f32[8]{0:T(128)S(1)}, f32[8]{0:T(128)}, u32[]{:S(2)}) copy-start(f32[8]{0:T(128)} %get-tuple-element.388) | copy-start | bytes 100
  422.6 20.6 %copy-start.46 = (f32[8]{0:T(128)S(1)}, f32[8]{0:T(128)}, u32[]{:S(2)}) copy-start(f32[8]{0:T(128)} %get-tuple-element.389) | copy-start | bytes 100
  422.7 20.6 %copy-start.47 = (f32[8]{0:T(128)S(1)}, f32[8]{0:T(128)}, u32[]{:S(2)}) copy-start(f32[8]{0:T(128)} %get-tuple-element.390) | copy-start | bytes 100
  422.7 20.6 %copy-start.49 = (f32[8]{0:T(128)S(1)}, f32[8]{0:T(128)}, u32[]{:S(2)}) copy-start(f32[8]{0:T(128)} %exponential_bitcast_fusion.8) | copy-start | bytes 100
  447.8 12.7 %copy-start.5 = (f32[768,8,64]{0,2,1:T(8,128)S(1)}, f32[768,8,64]{0,2,1:T(8,128)}, u32[]{:S(2)}) copy-start(f32[768,8,64]{0,2,1:T(8,128)} %reshape.898) | copy-start | bytes 4718596
  447.8 12.7 %copy-start.9 = (bf16[16,64,128]{2,1,0:T(8,128)(2,1)S(1)}, bf16[16,64,128]{2,1,0:T(8,128)(2,1)}, u32[]{:S(2)}) copy-start(bf16[16,64,128]{2,1,0:T(8,128)(2,1)} %copy-done.8) | copy-start | bytes 786436
  447.8 12.7 %copy-start.14 = (f32[768,8]{0,1:T(8,128)S(1)}, f32[768,8]{0,1:T(8,128)}, u32[]{:S(2)}) copy-start(f32[768,8]{0,1:T(8,128)} %exponential_bitcast_fusion.1) | copy-start | bytes 73732
  447.8 12.7 %copy-start.18 = (f32[8]{0:T(128)S(1)}, f32[8]{0:T(128)}, u32[]{:S(2)}) copy-start(f32[8]{0:T(128)} %get-tuple-element.401) | copy-start | bytes 100
  (25 other events, 219.7 us)
Sparse Core Ops, SparseCore 0:
  10.7 92.1 all-gather.11
  314.0 38.9 all-gather.15
  421.6 38.8 all-gather.13
where the time goes:
time: 528 us; the launch traced here: 523 us
  local copies, waits for them, and re-layouts  168 us (32%)
  blocking collectives  119 us (23%)
  waiting for transfers between devices  91.3 us (17%)
  matrix products  74.5 us (14%)
  other arithmetic  41 us (8%)
  between operations  15.4 us (3%)
  starting transfers between devices  11.2 us (2%)
    all_gather x1, waiting for transfers between devices, turned_gather(): out = lax.all_gather(both, axis, axis=0, tiled=True)  83.6 us
    all_gather x8, blocking collectives, carried_in(): lax.all_gather(part.astype(kind), axis)  79.8 us
    dynamic_update_slice x12, local copies, waits for them, and re-layouts, direction(): end_state, local = lax.scan(block_ssd, start_state, shaped)  76.7 us
    all_to_all x1, blocking collectives, sent_and_summed(): lax.all_to_all(parts, axis, split_axis=0, concat_axis=0, tiled=True)  36.8 us
    dynamic_slice x12, local copies, waits for them, and re-layouts, direction(): end_state, local = lax.scan(block_ssd, start_state, shaped)  22.4 us
    dot_general x5, matrix products, shards(): jnp.dot(normed, matrix, preferred_element_type=jnp.float32)  20.3 us
    another operation x20, local copies, waits for them, and re-layouts  18.8 us
    dot_general x12, matrix products, block_ssd(): jnp.einsum('lsh,shp->lhp', intersection * weight, xdt, precision=HIGH)  12.7 us
  transfers between devices with their start and end apart: 7, of which 2 were waited for; matrix products, arithmetic and copies ran while one was open for 49% of the time, Pallas kernels for 0%

commit v1 on v0

--- a/solution.py
+++ b/solution.py
@@ -20,7 +20,8 @@
     turned = [jnp.moveaxis(a, dim, 0) for a, dim in zip(arrays, dims)]
     widths = [t[0].size for t in turned]
     both = jnp.concatenate([t.reshape(-1, w) for t, w in zip(turned, widths)], axis=1)
-    out = lax.all_gather(both, axis, axis=0, tiled=True)
+    stack = jnp.stack([both] * lax.axis_size(axis))
+    out = jnp.concatenate(lax.all_to_all(stack, axis, 0, 0), axis=0)
     parts = jnp.split(out, [sum(widths[:k]) for k in range(1, len(widths))], axis=1)
     return tuple(
         (

time: 528 us -> 745 us (1.41)
  waiting for transfers between devices: 91.3 us -> 284 us
  starting transfers between devices: 11.2 us -> 23.6 us
    all_to_all x0 -> x1, waiting for transfers between devices: none -> 284 us  [turned_gather(): out = jnp.concatenate(lax.all_to_all(stack, axis, 0, 0), axis=0)]
    all_gather x1 -> x0, waiting for transfers between devices: 83.6 us -> none  [turned_gather(): out = lax.all_gather(both, axis, axis=0, tiled=True)]
    all_to_all x0 -> x1, starting transfers between devices: none -> 12.4 us  [turned_gather(): out = jnp.concatenate(lax.all_to_all(stack, axis, 0, 0), axis=0)]
    all_gather x2, waiting for transfers between devices: 7.54 us -> 0.01 us  [carried_in(): lax.all_gather(part.astype(kind), axis)]
    another operation x20 -> x21, local copies, waits for them, and re-layouts: 18.8 us -> 22.9 us
  transfers between devices with their start and end apart: 7 -> 7, of which waited for: 2 -> 1; matrix products, arithmetic and copies ran while one was open for 49% -> 33% of each run, Pallas kernels for 0% -> 0%
where the time goes in v1:
time: 745 us; the launch traced here: 738 us
  waiting for transfers between devices  284 us (38%)
  local copies, waits for them, and re-layouts  175 us (23%)
  blocking collectives  119 us (16%)
  matrix products  80.1 us (11%)
  other arithmetic  37.2 us (5%)
  starting transfers between devices  23.6 us (3%)
  between operations  15.8 us (2%)
    all_to_all x1, waiting for transfers between devices, turned_gather(): out = jnp.concatenate(lax.all_to_all(stack, axis, 0, 0), axis=0)  284 us
    all_gather x8, blocking collectives, carried_in(): lax.all_gather(part.astype(kind), axis)  78.3 us
    dynamic_update_slice x12, local copies, waits for them, and re-layouts, direction(): end_state, local = lax.scan(block_ssd, start_state, shaped)  76.8 us
    all_to_all x1, blocking collectives, sent_and_summed(): lax.all_to_all(parts, axis, split_axis=0, concat_axis=0, tiled=True)  38.5 us
    dynamic_slice x12, local copies, waits for them, and re-layouts, direction(): end_state, local = lax.scan(block_ssd, start_state, shaped)  22.6 us
    dot_general x5, matrix products, shards(): jnp.dot(normed, matrix, preferred_element_type=jnp.float32)  19.4 us
    another operation x20, local copies, waits for them, and re-layouts  17.3 us
  transfers between devices with their start and end apart: 7, of which 1 were waited for; matrix products, arithmetic and copies ran while one was open for 33% of the time, Pallas kernels for 0%

profile of v1, /device:TPU:8, one launch (start us, length us, event | category | flops | bytes accessed | tf_op | source)
XLA Modules:
  0.0 738.3 jit_solution(17940003640860717334)
XLA Ops:
  9.7 5.6 stack.2
  15.4 12.4 %all-to-all-start = ((bf16[64,32,3088]{2,1,0:T(8,128)(2,1)}), bf16[64,32,3088]{2,1,0:T(8,128)(2,1)}, u32[]{:S(2)}, u32[]{:S(2)}) async-start(bf16[64,32,3088]{2,1,0:T(8,128)(2,1)} %stack.2), calls=%async_computation | async-start | bytes 26214400 | tf_op jit(solution)/shard_map/all_to_all | solution.py:24
  32.9 283.9 %all-to-all-done = bf16[64,32,3088]{2,1,0:T(8,128)(2,1)} async-done(((bf16[64,32,3088]{2,1,0:T(8,128)(2,1)}), bf16[64,32,3088]{2,1,0:T(8,128)(2,1)}, u32[]{:S(2)}, u32[]{:S(2)}) %all-to-all-start) | async-done | bytes 12648480 | tf_op jit(solution)/shard_map/all_to_all | solution.py:24
  316.7 5.6 fusion.101
  322.4 4.6 fusion.107
  342.6 7.0 all-gather.4
  350.8 9.3 %all-gather.6 = bf16[4,1,8]{2,1,0:T(2,128)(2,1)S(1)} all-gather(bf16[1,1,8]{2,1,0:T(2,128)(2,1)S(1)} %get-tuple-element.405), channel_id=1, replica_groups=mesh['sp_0'=8,'sp_1'=4,'sp_2'=2,'tp'=4] {'sp_1'}, dimensions={0}, use_global_device_ids=true | all-gather | bytes 80 | tf_op jit(solution)/shard_map/all_gather | solution.py:46
  361.3 16.3 %all-gather.7 = bf16[8,1,8]{2,1,0:T(2,128)(2,1)S(1)} all-gather(bf16[1,1,8]{2,1,0:T(2,128)(2,1)S(1)} %get-tuple-element.396), channel_id=1, replica_groups=mesh['sp_0'=8,'sp_1'=4,'sp_2'=2,'tp'=4] {'sp_0'}, dimensions={0}, use_global_device_ids=true | all-gather | bytes 144 | tf_op jit(solution)/shard_map/all_gather | solution.py:46
  382.3 13.7 %all-gather.5 = bf16[8,1,8]{2,1,0:T(2,128)(2,1)S(1)} all-gather(bf16[1,1,8]{2,1,0:T(2,128)(2,1)S(1)} %get-tuple-element.391), channel_id=1, replica_groups=mesh['sp_0'=8,'sp_1'=4,'sp_2'=2,'tp'=4] {'sp_0'}, dimensions={0}, use_global_device_ids=true | all-gather | bytes 144 | tf_op jit(solution)/shard_map/all_gather | solution.py:46
  403.9 3.6 collective-permute-start.3
  430.4 74.5 %while.42 = (s32[]{:T(128)}, f32[8,64,128]{2,1,0:T(8,128)S(1)}, f32[6,128,8,64]{1,0,3,2:T(8,128)S(1)}, f32[6,128,8]{2,1,0:T(8,128)}, f32[6,128,8,64]{1,0,3,2:T(8...) while((s32[]{:T(128)}, f32[8,64,128]{2,1,0:T(8,128)S(1)}, ...), condition=%wide.region_9.10_spmd.clone, body=%wide.region_7.9_spmd.clone.sunk | while | flops 156188672 | bytes 3768644 | solution.py:231
  437.3 5.1 dynamic_update_slice.32
  449.7 5.1 dynamic_update_slice.32
  462.1 5.1 dynamic_update_slice.32
  474.5 5.1 dynamic_update_slice.32
  487.0 5.1 dynamic_update_slice.32
  499.4 5.1 dynamic_update_slice.32
  507.6 14.4 %all_gather.64 = bf16[4,8,64,128]{3,2,1,0:T(8,128)(2,1)S(1)} all-gather(bf16[1,8,64,128]{3,2,1,0:T(8,128)(2,1)S(1)} %fusion.172), channel_id=1, replica_groups=mesh['sp_0'=8,'sp_1'=4,'sp_2'=2,'tp'=4] {'sp_1'}, dimensions={0}, use_global_device_ids=true | all-gather | bytes 655360 | tf_op jit(solution)/shard_map/all_gather | solution.py:46
  529.0 80.3 %while.41 = (s32[]{:T(128)}, f32[8,64,128]{2,1,0:T(8,128)S(1)}, f32[6,128,8,64]{1,0,3,2:T(8,128)}, f32[6,128,8]{2,1,0:T(8,128)}, f32[6,128,8,64]{1,0,3,2:T(8,128...) while((s32[]{:T(128)}, f32[8,64,128]{2,1,0:T(8,128)S(1)}, ...), condition=%wide.region_3.4_spmd.clone, body=%wide.region_1.3_spmd.clone.sunk | while | flops 156188672 | bytes 3768644 | solution.py:231
  534.3 7.7 %dynamic_update_slice.31 = f32[6,128,8,64]{1,0,3,2:T(8,128)} dynamic-update-slice(f32[6,128,8,64]{1,0,3,2:T(8,128)} %get-tuple-element.665, f32[1,128,8,64]{1,0,3,2:T(1,128)S(1)} %bitcast.675, s32[]{:T(128)} %get-tuple-element.663, s32[]{:T(128)} %constant.172.clone.1..sunk.1, s32[]{:T(128)} %constant.172.clone.1..sunk.1, s32[]{:T(128)} %constant.172.clone.1..sunk.1) | dynamic-update-slice | bytes 524292 | tf_op jit(solution)/shard_map/while/body/jit(dynamic_update_index_in_dim)/dynamic_update_slice | solution.py:231
  547.7 7.7 %dynamic_update_slice.31 = f32[6,128,8,64]{1,0,3,2:T(8,128)} dynamic-update-slice(f32[6,128,8,64]{1,0,3,2:T(8,128)} %get-tuple-element.665, f32[1,128,8,64]{1,0,3,2:T(1,128)S(1)} %bitcast.675, s32[]{:T(128)} %get-tuple-element.663, s32[]{:T(128)} %constant.172.clone.1..sunk.1, s32[]{:T(128)} %constant.172.clone.1..sunk.1, s32[]{:T(128)} %constant.172.clone.1..sunk.1) | dynamic-update-slice | bytes 524292 | tf_op jit(solution)/shard_map/while/body/jit(dynamic_update_index_in_dim)/dynamic_update_slice | solution.py:231
  561.1 7.7 %dynamic_update_slice.31 = f32[6,128,8,64]{1,0,3,2:T(8,128)} dynamic-update-slice(f32[6,128,8,64]{1,0,3,2:T(8,128)} %get-tuple-element.665, f32[1,128,8,64]{1,0,3,2:T(1,128)S(1)} %bitcast.675, s32[]{:T(128)} %get-tuple-element.663, s32[]{:T(128)} %constant.172.clone.1..sunk.1, s32[]{:T(128)} %constant.172.clone.1..sunk.1, s32[]{:T(128)} %constant.172.clone.1..sunk.1) | dynamic-update-slice | bytes 524292 | tf_op jit(solution)/shard_map/while/body/jit(dynamic_update_index_in_dim)/dynamic_update_slice | solution.py:231
  574.5 7.7 %dynamic_update_slice.31 = f32[6,128,8,64]{1,0,3,2:T(8,128)} dynamic-update-slice(f32[6,128,8,64]{1,0,3,2:T(8,128)} %get-tuple-element.665, f32[1,128,8,64]{1,0,3,2:T(1,128)S(1)} %bitcast.675, s32[]{:T(128)} %get-tuple-element.663, s32[]{:T(128)} %constant.172.clone.1..sunk.1, s32[]{:T(128)} %constant.172.clone.1..sunk.1, s32[]{:T(128)} %constant.172.clone.1..sunk.1) | dynamic-update-slice | bytes 524292 | tf_op jit(solution)/shard_map/while/body/jit(dynamic_update_index_in_dim)/dynamic_update_slice | solution.py:231
  587.9 7.7 %dynamic_update_slice.31 = f32[6,128,8,64]{1,0,3,2:T(8,128)} dynamic-update-slice(f32[6,128,8,64]{1,0,3,2:T(8,128)} %get-tuple-element.665, f32[1,128,8,64]{1,0,3,2:T(1,128)S(1)} %bitcast.675, s32[]{:T(128)} %get-tuple-element.663, s32[]{:T(128)} %constant.172.clone.1..sunk.1, s32[]{:T(128)} %constant.172.clone.1..sunk.1, s32[]{:T(128)} %constant.172.clone.1..sunk.1) | dynamic-update-slice | bytes 524292 | tf_op jit(solution)/shard_map/while/body/jit(dynamic_update_index_in_dim)/dynamic_update_slice | solution.py:231
  601.3 7.7 %dynamic_update_slice.31 = f32[6,128,8,64]{1,0,3,2:T(8,128)} dynamic-update-slice(f32[6,128,8,64]{1,0,3,2:T(8,128)} %get-tuple-element.665, f32[1,128,8,64]{1,0,3,2:T(1,128)S(1)} %bitcast.675, s32[]{:T(128)} %get-tuple-element.663, s32[]{:T(128)} %constant.172.clone.1..sunk.1, s32[]{:T(128)} %constant.172.clone.1..sunk.1, s32[]{:T(128)} %constant.172.clone.1..sunk.1) | dynamic-update-slice | bytes 524292 | tf_op jit(solution)/shard_map/while/body/jit(dynamic_update_index_in_dim)/dynamic_update_slice | solution.py:231
  611.5 13.6 %all_gather.57 = bf16[4,8,64,128]{3,2,1,0:T(8,128)(2,1)S(1)} all-gather(bf16[1,8,64,128]{3,2,1,0:T(8,128)(2,1)S(1)} %fusion.168), channel_id=1, replica_groups=mesh['sp_0'=8,'sp_1'=4,'sp_2'=2,'tp'=4] {'sp_1'}, dimensions={0}, use_global_device_ids=true | all-gather | bytes 655360 | tf_op jit(solution)/shard_map/all_gather | solution.py:46
  631.5 31.5 %while.40 = (s32[]{:T(128)}, bf16[3,256,512]{2,1,0:T(8,128)(2,1)S(1)}, f32[3,256,8]{1,2,0:T(8,128)}, s32[3]{0:T(128)S(1)}, bf16[1024,256]{0,1:T(8,128)(2,1)S(1)}...) while((s32[]{:T(128)}, ...), condition=%wide.region_17.18_spmd, body=%wide.region_14.17_spmd.sunk | while | flops 280901888 | bytes 32392092 | solution.py:306
  664.4 4.4 fusion.98
  668.9 5.0 rev.16
  677.3 4.0 multiply_reduce_fusion
  682.5 8.7 %fusion.78 = bf16[768,2048]{1,0:T(8,128)(2,1)S(1)} fusion(bf16[2048,3088]{1,0:T(8,128)(2,1)} %bitcast.21, bf16[768,512]{0,1:T(8,128)(2,1)S(1)} %copy-done.12, bf16[768,512]{0,1:T(8,128)(2,1)S(1)} %multiply_convert_fusion.1), kind=kOutput, calls=%fused_computation.107 | convolution fusion | flops 3225944064 | bytes 8912896 | tf_op jit(solution)/shard_map/dot_general | solution.py:310
  691.4 38.5 %all_to_all.10 = bf16[4,768,512]{2,1,0:T(8,128)(2,1)S(1)} all-to-all(bf16[4,768,512]{2,1,0:T(8,128)(2,1)S(1)} %bitcast.678), channel_id=1, replica_groups=mesh['sp_0'=8,'sp_1'=4,'sp_2'=2,'tp'=4] {'tp'}, dimensions={0} | all-to-all | bytes 6291456 | tf_op jit(solution)/shard_map/all_to_all | solution.py:86
  (473 shorter events, 192.0 us)
Async XLA Ops:
  15.4 301.3 %all-to-all-start = ((bf16[64,32,3088]{2,1,0:T(8,128)(2,1)}), bf16[64,32,3088]{2,1,0:T(8,128)(2,1)}, u32[]{:S(2)}, u32[]{:S(2)}) async-start(bf16[64,32,3088]{2,1,0:T(8,128)(2,1)} %stack.2), calls=%async_computation | async-start | bytes 26214400 | tf_op jit(solution)/shard_map/all_to_all | solution.py:24
  27.8 636.4 %all-gather.13.cloned.1.call-start = ((), (), s32[]{:S(2)}) async-start(), calls=%async_computation.3 | async-start | bytes 1179648 | tf_op jit(solution)/shard_map/all_gather | solution.py:46
  32.4 303.2 %copy-start.21 = (f32[768]{0:T(1024)}, f32[768]{0:T(1024)S(1)}, u32[]{:S(2)}) copy-start(f32[768]{0:T(1024)S(1)} %add_rsqrt_fusion.1) | copy-start | bytes 9220
  330.1 80.3 %collective-permute-start = (bf16[2,768]{1,0:T(2,128)(2,1)S(1)}, bf16[2,768]{1,0:T(2,128)(2,1)S(1)}, u32[]{:S(2)}, u32[]{:S(2)}) collective-permute-start(bf16[2,768]{1,0:T(2,128)(2,1)S(1)} %get-tuple-element.353), channel_id=1, source_target_pairs={{0,4},{4,8},{8,12},{12,16},{16,20},{20,24},{24,28},{28,32},{32,36}... | collective-permute-start | bytes 9224 | tf_op jit(solution)/shard_map/ppermute | solution.py:69
  332.0 78.4 %collective-permute-start.1 = (bf16[2,768]{1,0:T(2,128)(2,1)S(1)}, bf16[2,768]{1,0:T(2,128)(2,1)S(1)}, u32[]{:S(2)}, u32[]{:S(2)}) collective-permute-start(bf16[2,768]{1,0:T(2,128)(2,1)S(1)} %get-tuple-element.354), channel_id=1, source_target_pairs={{4,0},{8,4},{12,8},{16,12},{20,16},{24,20},{28,24},{32,28},{36,32}... | collective-permute-start | bytes 9224 | tf_op jit(solution)/shard_map/ppermute | solution.py:71
  401.9 228.4 %collective-permute-start.2 = (bf16[128,256]{0,1:T(8,128)(2,1)}, bf16[128,256]{0,1:T(8,128)(2,1)}, u32[]{:S(2)}, u32[]{:S(2)}) collective-permute-start(bf16[128,256]{0,1:T(8,128)(2,1)} %get-tuple-element.359), channel_id=1, source_target_pairs={{0,4},{4,8},{8,12},{12,16},{16,20},{20,24},{24,28},{28,32},{32,36}... | collective-permute-start | bytes 196616 | tf_op jit(solution)/shard_map/ppermute | solution.py:69
  403.9 226.5 %collective-permute-start.3 = (bf16[128,256]{0,1:T(8,128)(2,1)}, bf16[128,256]{0,1:T(8,128)(2,1)}, u32[]{:S(2)}, u32[]{:S(2)}) collective-permute-start(bf16[128,256]{0,1:T(8,128)(2,1)} %get-tuple-element.360), channel_id=1, source_target_pairs={{4,0},{8,4},{12,8},{16,12},{20,16},{24,20},{28,24},{32,28},{36,32}... | collective-permute-start | bytes 196616 | tf_op jit(solution)/shard_map/ppermute | solution.py:71
  524.4 149.5 %all-gather.11.cloned.1.call-start = ((), (), s32[]{:S(2)}) async-start(), calls=%async_computation.2 | async-start | bytes 1179648 | tf_op jit(solution)/shard_map/all_gather | solution.py:46
  529.0 82.4 %copy-start.23 = (f32[8]{0:T(128)S(1)}, f32[8]{0:T(128)}, u32[]{:S(2)}) copy-start(f32[8]{0:T(128)} %get-tuple-element.401) | copy-start | bytes 100
  529.0 82.4 %copy-start.24 = (f32[8]{0:T(128)S(1)}, f32[8]{0:T(128)}, u32[]{:S(2)}) copy-start(f32[8]{0:T(128)} %get-tuple-element.403) | copy-start | bytes 100
  529.0 96.2 %copy-start.25 = (f32[8]{0:T(128)S(1)}, f32[8]{0:T(128)}, u32[]{:S(2)}) copy-start(f32[8]{0:T(128)} %get-tuple-element.392) | copy-start | bytes 100
  529.0 96.2 %copy-start.29 = (f32[8]{0:T(128)S(1)}, f32[8]{0:T(128)}, u32[]{:S(2)}) copy-start(f32[8]{0:T(128)} %get-tuple-element.393) | copy-start | bytes 100
  529.0 96.2 %copy-start.30 = (f32[8]{0:T(128)S(1)}, f32[8]{0:T(128)}, u32[]{:S(2)}) copy-start(f32[8]{0:T(128)} %get-tuple-element.394) | copy-start | bytes 100
  529.0 96.1 %copy-start.31 = (f32[8]{0:T(128)S(1)}, f32[8]{0:T(128)}, u32[]{:S(2)}) copy-start(f32[8]{0:T(128)} %get-tuple-element.395) | copy-start | bytes 100
  631.3 32.9 %copy-start.10 = (bf16[16,64,128]{2,1,0:T(8,128)(2,1)S(1)}, bf16[16,64,128]{2,1,0:T(8,128)(2,1)}, u32[]{:S(2)}) copy-start(bf16[16,64,128]{2,1,0:T(8,128)(2,1)} %copy-done.9) | copy-start | bytes 786436
  631.3 32.9 %copy-start.14 = (bf16[6,128,1,128]{3,1,2,0:T(8,128)(2,1)S(1)}, bf16[6,128,1,128]{3,1,2,0:T(8,128)(2,1)}, u32[]{:S(2)}) copy-start(bf16[6,128,1,128]{3,1,2,0:T(8,128)(2,1)} %copy-done.13) | copy-start | bytes 589828
  631.4 32.9 %copy-start.17 = (f32[768,8]{0,1:T(8,128)S(1)}, f32[768,8]{0,1:T(8,128)}, u32[]{:S(2)}) copy-start(f32[768,8]{0,1:T(8,128)} %exponential_bitcast_fusion) | copy-start | bytes 73732
  631.4 32.9 %copy-start.26 = (f32[8]{0:T(128)S(1)}, f32[8]{0:T(128)}, u32[]{:S(2)}) copy-start(f32[8]{0:T(128)} %get-tuple-element.404) | copy-start | bytes 100
  631.4 32.9 %copy-start.27 = (f32[8]{0:T(128)S(1)}, f32[8]{0:T(128)}, u32[]{:S(2)}) copy-start(f32[8]{0:T(128)} %get-tuple-element.406) | copy-start | bytes 100
  631.4 32.9 %copy-start.28 = (f32[8]{0:T(128)S(1)}, f32[8]{0:T(128)}, u32[]{:S(2)}) copy-start(f32[8]{0:T(128)} %get-tuple-element.397) | copy-start | bytes 100
  631.4 32.9 %copy-start.32 = (f32[8]{0:T(128)S(1)}, f32[8]{0:T(128)}, u32[]{:S(2)}) copy-start(f32[8]{0:T(128)} %get-tuple-element.398) | copy-start | bytes 100
  631.4 32.9 %copy-start.33 = (f32[8]{0:T(128)S(1)}, f32[8]{0:T(128)}, u32[]{:S(2)}) copy-start(f32[8]{0:T(128)} %get-tuple-element.399) | copy-start | bytes 100
  631.4 32.9 %copy-start.34 = (f32[8]{0:T(128)S(1)}, f32[8]{0:T(128)}, u32[]{:S(2)}) copy-start(f32[8]{0:T(128)} %get-tuple-element.400) | copy-start | bytes 100
  631.4 32.9 %copy-start.47 = (f32[8]{0:T(128)S(1)}, f32[8]{0:T(128)}, u32[]{:S(2)}) copy-start(f32[8]{0:T(128)} %get-tuple-element.329) | copy-start | bytes 100
  631.4 32.9 %copy-start.48 = (f32[8]{0:T(128)S(1)}, f32[8]{0:T(128)}, u32[]{:S(2)}) copy-start(f32[8]{0:T(128)} %get-tuple-element.383) | copy-start | bytes 100
  631.4 32.9 %copy-start.49 = (f32[8]{0:T(128)S(1)}, f32[8]{0:T(128)}, u32[]{:S(2)}) copy-start(f32[8]{0:T(128)} %get-tuple-element.384) | copy-start | bytes 100
  631.5 32.9 %copy-start.50 = (f32[8]{0:T(128)S(1)}, f32[8]{0:T(128)}, u32[]{:S(2)}) copy-start(f32[8]{0:T(128)} %get-tuple-element.385) | copy-start | bytes 100
  631.5 32.9 %copy-start.51 = (f32[8]{0:T(128)S(1)}, f32[8]{0:T(128)}, u32[]{:S(2)}) copy-start(f32[8]{0:T(128)} %get-tuple-element.386) | copy-start | bytes 100
  631.5 32.9 %copy-start.52 = (f32[8]{0:T(128)S(1)}, f32[8]{0:T(128)}, u32[]{:S(2)}) copy-start(f32[8]{0:T(128)} %get-tuple-element.387) | copy-start | bytes 100
  631.5 32.9 %copy-start.53 = (f32[8]{0:T(128)S(1)}, f32[8]{0:T(128)}, u32[]{:S(2)}) copy-start(f32[8]{0:T(128)} %get-tuple-element.388) | copy-start | bytes 100
  631.5 32.9 %copy-start.54 = (f32[8]{0:T(128)S(1)}, f32[8]{0:T(128)}, u32[]{:S(2)}) copy-start(f32[8]{0:T(128)} %get-tuple-element.389) | copy-start | bytes 100
  631.5 32.9 %copy-start.55 = (f32[8]{0:T(128)S(1)}, f32[8]{0:T(128)}, u32[]{:S(2)}) copy-start(f32[8]{0:T(128)} %get-tuple-element.390) | copy-start | bytes 100
  (38 other events, 296.6 us)
Sparse Core Ops, SparseCore 0:
  524.5 39.0 all-gather.12
  630.4 39.2 all-gather.10
